TPU v7x, 512 devices: a whole 4x8x8 slice. The times are simulated.
512 devices in a mesh: sp: 32 (over z, x), tp: 16 (over y, core).
Axes of the slice: x: 4, y: 8, z: 8, core: 2. Of those that a mesh axis runs over, the one named last changes fastest.
Arguments:
- skip_stream_entering: bfloat16 [4096, 2048], P('sp', 'tp'), may hold values from -24 to 24
- unfiltered_channel_feed: bfloat16 [4096, 2048], P('sp', 'tp'), may hold values from -6 to 6
- unfiltered_state_entry: bfloat16 [4096, 2048], P('sp', 'tp'), may hold values from -6 to 6
- unfiltered_state_exit: bfloat16 [4096, 2048], P('sp', 'tp'), may hold values from -6 to 6
- final_valve_preactivation: bfloat16 [4096, 2048], P('sp', 'tp'), may hold values from -6 to 6
- increment_preactivation: float32 [2, 32, 4096], P(None, 'tp', 'sp'), may hold values from -8 to 8
- summed_attenuation_both_ways: float32 [2, 32, 4096], P(None, 'tp', 'sp'), may hold values from -0.7 to 0, as said below
- channel_fading_speed: float32 [2, 32], P(None, 'tp'), may hold values from 4.8828125e-05 to 0.03, as said below
- channel_feed_filter: float32 [5, 2048], P(None, 'tp'), may hold values from -2.5 to 2.5
- state_entry_filter: float32 [5, 2048], P(None, 'tp'), may hold values from -2.5 to 2.5
- state_exit_filter: float32 [5, 2048], P(None, 'tp'), may hold values from -2.5 to 2.5
- clustered_rescale_factor: float32 [2048], P('tp'), may hold values from 0.1 to 1.9
- final_projection_weights: bfloat16 [2048, 2048], P(None, 'tp'), may hold values from -0.125 to 0.125
- specialist_rescale_factor: float32 [2048], replicated, may hold values from 0.1 to 1.9
- item_specialist_couple: int32 [4096, 2], P('sp'), may hold values from 0 to 31, all different within a row; in each aligned block of 128 rows (0 to 127, 128 to 255, ...) at most 16 rows name the same one
- selected_cluster_likelihood: float32 [4096], P('sp'), may hold values from 0.3 to 1
- selected_twin_scores_raw: float32 [4096, 2], P('sp'), may hold values from -6 to 6
- specialist_gating_weights: bfloat16 [32, 2048, 4096], P('sp', None, 'tp'), may hold values from -0.125 to 0.125
- specialist_raising_weights: bfloat16 [32, 2048, 4096], P('sp', None, 'tp'), may hold values from -0.125 to 0.125
- specialist_lowering_weights: bfloat16 [32, 4096, 2048], P('sp', 'tp'), may hold values from -0.09375 to 0.09375
Outputs:
- layer_out: bfloat16 [4096, 2048], P('sp', 'tp')
Inputs may be any that keep to these rules, and one draw needn't show every extreme that they name: For every head, dt times channel_fading_speed at the rate of the draw sets how far a state is carried; summed_attenuation_both_ways holds a few sharp losses of state. `summed_attenuation_both_ways`: mostly zero. `item_specialist_couple`: the two experts of a row differ. Among the rows of one index of sp (aligned blocks of 128 rows) no expert is named by more than 16 rows, a bound that some expert reaches in some blocks.
All inputs are finite; a program needn't handle non-finite values.
Results may differ from a plain program's by a relative error of at most 0.0095.
Values may be sent and summed in bfloat16 or wider, within the bound.
No kernel may reach another device: no remote copies, remote signals or barrier semaphores. Data moves between devices by JAX's collectives and lax.ppermute only.
A program may use at most 64 MiB of HBM per device.

v0:
```python
import jax
import jax.numpy as jnp
from jax import lax
from jax.sharding import Mesh
from jax.sharding import PartitionSpec as P

D = 2048
HD = 64
NS = 128
CONV = 5
SP = ("sp_0", "sp_1")
HIGHEST = lax.Precision.HIGHEST
group_eps = 1e-05
stream_eps = 1e-06


def extended(cells, sides, width):
    for axis, dim in sides:
        count = lax.axis_size(axis)
        ends = count - 1
        head = lax.slice_in_dim(cells, 0, width, axis=dim)
        tail = lax.slice_in_dim(cells, cells.shape[dim] - width, cells.shape[dim], axis=dim)
        cells = jnp.concatenate(
            [
                lax.ppermute(tail, axis, [(i, (i + 1) % count) for i in range(ends)]),
                cells,
                lax.ppermute(head, axis, [((i + 1) % count, i) for i in range(ends)]),
            ],
            axis=dim,
        )
    return cells


def filled_with(shard, identity):
    return jax.tree.map(
        lambda a, e: jnp.broadcast_to(jnp.asarray(e, a.dtype), a.shape), shard, identity
    )


def all_in_one(shard, axis):
    leaves = jax.tree.leaves(shard)
    sequence = sorted(range(len(leaves)), key=lambda k: -leaves[k].size)
    width = (1, *leaves[sequence[0]].shape)[-1]
    lines = [
        jnp.pad(leaves[k].reshape(-1), (0, -leaves[k].size % width)).reshape(-1, width)
        for k in sequence
    ]
    both, at, found = (lax.all_gather(jnp.concatenate(lines), axis), 0, {})
    for k, line in zip(sequence, lines):
        share = both[:, at : at + len(line)].reshape(len(both), -1)
        found[k] = share[:, : leaves[k].size].reshape(-1, *leaves[k].shape)
        at += len(line)
    numbers = iter(range(len(leaves)))
    return jax.tree.map(lambda _: found[next(numbers)], shard)


def carried_in(shard, axes, combine, identity, reverse):
    before = start = filled_with(shard, identity)
    so_far = shard
    for axis in reversed(axes):
        peers, mine = (lax.axis_size(axis), lax.axis_index(axis))
        pieces = all_in_one(
            jax.tree.map(
                lambda part, kind: part.astype(kind), so_far, (jnp.bfloat16, jnp.bfloat16)
            ),
            axis,
        )
        inside, so_far = (start, start)
        for k in reversed(range(peers)) if reverse else range(peers):
            passed = k > mine if reverse else k < mine
            so_far = combine(
                so_far, jax.tree.map(lambda part, own: part[k].astype(own.dtype), pieces, shard)
            )
            inside = jax.tree.map(lambda new, old: jnp.where(passed, new, old), so_far, inside)
        before = combine(inside, before)
    return before


def in_blocks(shard, dim, peers):
    shape = shard.shape
    parts = shard.reshape(*shape[:dim], peers, shape[dim] // peers, *shape[dim + 1 :])
    return jnp.moveaxis(parts, dim, 0)


def sum_at_owner(shard, axis, dim):
    peers = lax.axis_size(axis)
    parts = lax.all_to_all(in_blocks(shard, dim, peers), axis, 0, 0, tiled=True)
    return jnp.sum(parts.astype(jnp.float32), axis=0)


def block_parts(x_short, b_short, c_short, step_f, step_b, log_f, log_b):
    head_count = x_short.shape[1]
    group_count = b_short.shape[1]
    per_group = head_count // group_count
    length = x_short.shape[0]
    group_scores = jnp.einsum("tgn,sgn->gts", c_short, b_short, preferred_element_type=jnp.float32)
    x_block = x_short.astype(jnp.float32)
    b_block = b_short.astype(jnp.float32)
    c_block = c_short.astype(jnp.float32)
    scores = jnp.repeat(group_scores, per_group, axis=0)
    b_head = jnp.repeat(b_block, per_group, axis=1)
    c_head = jnp.repeat(c_block, per_group, axis=1)
    forward = jnp.cumsum(log_f, axis=1)
    backward = jnp.flip(jnp.cumsum(jnp.flip(log_b, 1), axis=1), 1)
    row_index = lax.broadcasted_iota(jnp.int32, (length, length), 0)
    col_index = lax.broadcasted_iota(jnp.int32, (length, length), 1)
    lower_mask = (col_index <= row_index)[None]
    upper_mask = (col_index >= row_index)[None]
    decay_fwd = jnp.where(
        lower_mask, jnp.exp(jnp.minimum(forward[:, :, None] - forward[:, None, :], 0.0)), 0.0
    )
    decay_bwd = jnp.where(
        upper_mask, jnp.exp(jnp.minimum(backward[:, :, None] - backward[:, None, :], 0.0)), 0.0
    )
    mixing = scores * (decay_fwd * step_f[:, None, :] + decay_bwd * step_b[:, None, :])
    within = jnp.einsum("hts,shp->thp", mixing, x_block, precision=HIGHEST)
    weight_fwd = jnp.exp(forward[:, -1:] - forward) * step_f
    weight_bwd = jnp.exp(backward[:, :1] - backward) * step_b
    state_fwd = jnp.einsum("hs,shp,shn->hpn", weight_fwd, x_block, b_head, precision=HIGHEST)
    state_bwd = jnp.einsum("hs,shp,shn->hpn", weight_bwd, x_block, b_head, precision=HIGHEST)
    return (
        within,
        state_fwd,
        state_bwd,
        forward[:, -1],
        backward[:, 0],
        jnp.exp(forward),
        jnp.exp(backward),
        c_head,
    )


def read_state(c_head, factor, state):
    return (
        jnp.einsum("thn,hpn->thp", c_head, state, precision=HIGHEST)
        * jnp.transpose(factor)[:, :, None]
    )


def compose(earlier, later):
    return (earlier[0] + later[0], earlier[1] * jnp.exp(later[0])[:, None, None] + later[1])


def body(
    skip_stream_entering,
    unfiltered_channel_feed,
    unfiltered_state_entry,
    unfiltered_state_exit,
    final_valve_preactivation,
    increment_preactivation,
    summed_attenuation_both_ways,
    channel_fading_speed,
    channel_feed_filter,
    state_entry_filter,
    state_exit_filter,
    clustered_rescale_factor,
    final_projection_weights,
    specialist_rescale_factor,
    item_specialist_couple,
    selected_cluster_likelihood,
    selected_twin_scores_raw,
    specialist_gating_weights,
    specialist_raising_weights,
    specialist_lowering_weights,
):
    tokens_here = skip_stream_entering.shape[0]
    heads_here = increment_preactivation.shape[1]
    x_width = unfiltered_channel_feed.shape[1]
    b_width = unfiltered_state_entry.shape[1]
    groups_here = b_width // NS
    joined = jnp.concatenate(
        [unfiltered_channel_feed, unfiltered_state_entry, unfiltered_state_exit], axis=1
    )
    padded = extended(joined, ((SP, 0),), CONV // 2)
    kernel = jnp.concatenate([channel_feed_filter, state_entry_filter, state_exit_filter], axis=1)
    summed = jnp.zeros(joined.shape, jnp.float32)
    for offset in range(CONV):
        summed = summed + kernel[offset] * padded[offset : offset + tokens_here].astype(jnp.float32)
    conv_out = jax.nn.silu(summed).astype(jnp.bfloat16)
    x_conv = conv_out[:, :x_width].reshape(tokens_here, heads_here, HD)
    b_conv = conv_out[:, x_width : x_width + b_width].reshape(tokens_here, groups_here, NS)
    c_conv = conv_out[:, x_width + b_width :].reshape(tokens_here, groups_here, NS)
    whole_increment_list = jax.nn.softplus(increment_preactivation)
    whole_attenuation_list = (
        -whole_increment_list * channel_fading_speed[:, :, None] + summed_attenuation_both_ways
    )
    within, state_fwd, state_bwd, total_fwd, total_bwd, factor_fwd, factor_bwd, c_head = (
        block_parts(
            x_conv,
            b_conv,
            c_conv,
            whole_increment_list[0],
            whole_increment_list[1],
            whole_attenuation_list[0],
            whole_attenuation_list[1],
        )
    )
    empty = (jnp.zeros_like(total_fwd), jnp.zeros_like(state_fwd))
    incoming_fwd = carried_in((total_fwd, state_fwd), SP, compose, empty, False)[1]
    incoming_bwd = carried_in((total_bwd, state_bwd), SP, compose, empty, True)[1]
    mixer_out = (
        within
        + read_state(c_head, factor_fwd, incoming_fwd)
        + read_state(c_head, factor_bwd, incoming_bwd)
    )
    gated = mixer_out.reshape(tokens_here, x_width) * jax.nn.silu(
        final_valve_preactivation.astype(jnp.float32)
    )
    grouped = gated.reshape(tokens_here, groups_here, -1)
    grouped = grouped * lax.rsqrt(jnp.mean(grouped * grouped, axis=-1, keepdims=True) + group_eps)
    mixed = (grouped.reshape(tokens_here, x_width) * clustered_rescale_factor).astype(jnp.bfloat16)
    projected = jnp.dot(
        lax.all_gather(mixed, "tp", axis=1, tiled=True),
        final_projection_weights,
        preferred_element_type=jnp.float32,
    )
    stream = (skip_stream_entering.astype(jnp.float32) + projected).astype(jnp.bfloat16)
    stream_f = stream.astype(jnp.float32)
    col_count = skip_stream_entering.shape[1]
    whole_rows = lax.all_gather(stream, "tp", axis=1, tiled=True).astype(jnp.float32)
    normal_rows = (
        whole_rows
        * lax.rsqrt(jnp.mean(whole_rows * whole_rows, axis=-1, keepdims=True) + stream_eps)
        * specialist_rescale_factor
    ).astype(jnp.bfloat16)
    expert_total = lax.axis_size(SP)
    capacity = 4 * tokens_here // expert_total
    flat_ids = item_specialist_couple.reshape(-1)
    assignments = flat_ids.shape[0]
    expert_iota = lax.broadcasted_iota(jnp.int32, (assignments, expert_total), 1)
    one_hot = (flat_ids[:, None] == expert_iota).astype(jnp.int32)
    ranking = jnp.sum((jnp.cumsum(one_hot, axis=0) - 1) * one_hot, axis=1)
    slot_index = flat_ids * capacity + ranking
    slot_iota = lax.broadcasted_iota(jnp.int32, (expert_total * capacity, assignments), 0)
    selector = (slot_index[None, :] == slot_iota).astype(jnp.bfloat16)
    selector = jnp.sum(selector.reshape(expert_total * capacity, tokens_here, -1), axis=2)
    weight_gate = specialist_gating_weights[0]
    weight_up = specialist_raising_weights[0]
    weight_down = specialist_lowering_weights[0]
    outgoing = jnp.dot(selector, normal_rows, preferred_element_type=jnp.float32).astype(
        jnp.bfloat16
    )
    outgoing = outgoing.reshape(expert_total, capacity, D)
    arrived = lax.all_to_all(outgoing, SP, split_axis=0, concat_axis=0, tiled=True)
    sources = arrived.shape[0]
    slot_count = arrived.shape[1]
    rows = arrived.reshape(sources * slot_count, arrived.shape[2])
    gate = jnp.dot(rows, weight_gate, preferred_element_type=jnp.float32)
    upward = jnp.dot(rows, weight_up, preferred_element_type=jnp.float32)
    hidden = (jax.nn.silu(gate) * upward).astype(jnp.bfloat16)
    partial_out = jnp.dot(hidden, weight_down, preferred_element_type=jnp.float32).astype(
        jnp.bfloat16
    )
    partial_out = partial_out.reshape(sources, slot_count, partial_out.shape[1])
    expert_cols = sum_at_owner(partial_out, "tp", 2).astype(jnp.bfloat16)
    returned = lax.all_to_all(expert_cols, SP, split_axis=0, concat_axis=0, tiled=True)
    flat_back = returned.reshape(expert_total * capacity, col_count)
    picked = (
        jnp.take(flat_back, slot_index, axis=0)
        .astype(jnp.float32)
        .reshape(tokens_here, -1, col_count)
    )
    first = jax.nn.sigmoid(selected_twin_scores_raw[:, 0] - selected_twin_scores_raw[:, 1])
    route_weight = selected_cluster_likelihood[:, None] * jnp.stack([first, 1.0 - first], axis=1)
    experts_sum = jnp.sum(route_weight[:, :, None] * picked, axis=1)
    return (stream_f + experts_sum).astype(jnp.bfloat16)


def solution(mesh):
    torus = Mesh(mesh.devices.reshape(8, 4, mesh.shape["tp"]), ("sp_0", "sp_1", "tp"))
    return jax.shard_map(
        body,
        mesh=torus,
        in_specs=(
            P(SP, "tp"),
            P(SP, "tp"),
            P(SP, "tp"),
            P(SP, "tp"),
            P(SP, "tp"),
            P(None, "tp", SP),
            P(None, "tp", SP),
            P(None, "tp"),
            P(None, "tp"),
            P(None, "tp"),
            P(None, "tp"),
            P("tp"),
            P(None, "tp"),
            P(),
            P(SP, None),
            P(SP),
            P(SP, None),
            P(SP, None, "tp"),
            P(SP, None, "tp"),
            P(SP, "tp", None),
        ),
        out_specs=P(SP, "tp"),
        check_vma=False,
    )
```

profile of v0, /device:TPU:1, one launch (start us, length us, event | category | flops | bytes accessed | tf_op | source)
XLA Modules:
  0.0 280.2 jit_solution(5651927392031734438)
XLA Ops:
  0.0 0.9 constant_dynamic-update-slice_fusion.5
  0.9 0.8 constant_dynamic-update-slice_fusion.4
  1.6 0.8 constant_dynamic-update-slice_fusion.3
  2.4 3.9 %collective-permute-start = (bf16[2,384]{1,0:T(2,128)(2,1)S(1)}, bf16[2,384]{1,0:T(2,128)(2,1)S(1)}, u32[]{:S(2)}, u32[]{:S(2)}) collective-permute-start(bf16[2,384]{1,0:T(2,128)(2,1)S(1)} %get-tuple-element.47), channel_id=1, source_target_pairs={{0,16},{16,32},{32,48},{48,64},{64,80},{80,96},{96,112},{112,128},... | collective-permute-start | bytes 4616 | tf_op jit(solution)/shard_map/ppermute | solution.py:25
  6.3 1.3 collective-permute-start.1
  7.7 0.8 copy.71
  8.5 0.1 eq.27
  8.6 0.1 reshape.638
  8.8 0.8 multiply_add_fusion
  9.5 0.1 rev.7
  9.6 0.3 reduce_window_sum.30
  9.9 0.3 reduce_window_sum.31
  10.3 0.1 rev.8
  10.3 0.2 slice_reduce_fusion.6
  10.7 0.7 constant_dynamic-update-slice_fusion.2
  11.4 0.7 constant_dynamic-update-slice_fusion.1
  12.1 0.7 constant_dynamic-update-slice_fusion
  12.8 0.6 reduce-window.6
  13.4 0.2 slice_reduce_fusion
  13.6 0.1 fusion.128
  13.7 0.1 reduce_sum.66
  14.0 0.7 compare_and_fusion
  14.8 0.2 multiply_convert_fusion
  15.0 0.1 copy.66
  15.1 0.2 convolution_convert_fusion.2
  15.4 10.4 %all-gather.6 = bf16[4,129,128]{2,1,0:T(8,128)(2,1)S(1)} all-gather(bf16[1,129,128]{2,1,0:T(8,128)(2,1)S(1)} %maximum_bitcast_fusion.2), channel_id=4, replica_groups=mesh['sp_0'=8,'sp_1'=4,'tp'=16] {'sp_1'}, dimensions={0}, use_global_device_ids=true | all-gather | bytes 165120 | tf_op jit(solution)/shard_map/all_gather | solution.py:48
  26.0 0.1 mul.547
  26.3 0.1 mul.555
  26.4 0.1 fusion.71
  26.6 27.4 %all-gather.7 = bf16[8,129,128]{2,1,0:T(8,128)(2,1)S(1)} all-gather(bf16[1,129,128]{2,1,0:T(8,128)(2,1)S(1)} %maximum_bitcast_fusion.3), channel_id=5, replica_groups=mesh['sp_0'=8,'sp_1'=4,'tp'=16] {'sp_0'}, dimensions={0}, use_global_device_ids=true | all-gather | bytes 297216 | tf_op jit(solution)/shard_map/all_gather | solution.py:48
  54.0 0.2 convolution_convert_fusion.3
  54.2 9.1 %all-gather.4 = bf16[4,129,128]{2,1,0:T(8,128)(2,1)S(1)} all-gather(bf16[1,129,128]{2,1,0:T(8,128)(2,1)S(1)} %maximum_bitcast_fusion), channel_id=2, replica_groups=mesh['sp_0'=8,'sp_1'=4,'tp'=16] {'sp_1'}, dimensions={0}, use_global_device_ids=true | all-gather | bytes 165120 | tf_op jit(solution)/shard_map/all_gather | solution.py:48
  63.6 0.1 mul.504
  64.0 0.1 fusion.75
  64.2 18.5 %all-gather.5 = bf16[8,129,128]{2,1,0:T(8,128)(2,1)S(1)} all-gather(bf16[1,129,128]{2,1,0:T(8,128)(2,1)S(1)} %maximum_bitcast_fusion.1), channel_id=3, replica_groups=mesh['sp_0'=8,'sp_1'=4,'tp'=16] {'sp_0'}, dimensions={0}, use_global_device_ids=true | all-gather | bytes 297216 | tf_op jit(solution)/shard_map/all_gather | solution.py:48
  82.8 0.1 fusion.184
  83.0 0.4 convolution_bitcast_fusion.2
  83.4 0.5 fusion.5
  83.9 0.5 fusion.3
  84.5 0.1 copy.69
  84.6 0.1 multiply_reduce_fusion.1
  84.7 0.1 multiply_convert_fusion.1
  84.8 37.9 %all_gather.38 = bf16[128,2048]{1,0:T(8,128)(2,1)S(1)} all-gather(bf16[128,128]{1,0:T(8,128)(2,1)S(1)} %multiply_convert_fusion.1), channel_id=1, replica_groups=mesh['sp_0'=8,'sp_1'=4,'tp'=16] {'tp'}, dimensions={1}, use_global_device_ids=true | all-gather | bytes 557056 | tf_op jit(solution)/shard_map/all_gather | solution.py:213
  122.7 0.3 fusion.6
  123.0 16.4 %all_gather.39 = bf16[128,2048]{1,0:T(8,128)(2,1)S(1)} all-gather(bf16[128,128]{1,0:T(8,128)(2,1)S(1)} %fusion.6), channel_id=1, replica_groups=mesh['sp_0'=8,'sp_1'=4,'tp'=16] {'tp'}, dimensions={1}, use_global_device_ids=true | all-gather | bytes 557056 | tf_op jit(solution)/shard_map/all_gather | solution.py:220
  139.4 0.2 fusion.7
  139.6 0.8 convolution_convert_fusion.1
  140.4 55.6 %all_to_all.15 = bf16[32,16,2048]{2,1,0:T(8,128)(2,1)S(1)} all-to-all(bf16[32,16,2048]{2,1,0:T(8,128)(2,1)S(1)} %bitcast.252), channel_id=1, replica_groups=mesh['sp_0'=8,'sp_1'=4,'tp'=16] {'sp_0','sp_1'}, dimensions={0} | all-to-all | bytes 4194304 | tf_op jit(solution)/shard_map/all_to_all | solution.py:244
  196.0 1.5 fusion.12
  197.5 5.0 %fusion = bf16[64,8,16,128]{3,1,2,0:T(8,128)(2,1)} fusion(bf16[1,256,2048]{2,1,0:T(8,128)(2,1)S(1)} %copy-done, bf16[512,2048]{1,0:T(8,128)(2,1)S(1)} %bitcast.256, bf16[1,2048,256]{2,1,0:T(8,128)(2,1)} %param.38, f32[512,256]{1,0:T(8,128)} %fusion.12), kind=kOutput, calls=%fused_computation.4 | convolution fusion | flops 1075576832 | bytes 6815744 | tf_op jit(solution)/shard_map/dot_general | solution.py:251
  202.6 2.2 copy.83
  204.8 1.9 copy.90
  206.7 6.9 %all-to-all-start.1 = ((bf16[16,32,16,128]{3,2,1,0:T(8,128)(2,1)}), bf16[16,32,16,128]{3,2,1,0:T(8,128)(2,1)S(1)}, u32[]{:S(2)}, u32[]{:S(2)}) async-start(bf16[16,32,16,128]{3,2,1,0:T(8,128)(2,1)} %bitcast.251), calls=%async_computation.1 | async-start | bytes 4194304 | tf_op jit(solution)/shard_map/all_to_all | solution.py:87
  213.6 0.1 copy.77
  213.7 0.1 mul.604
  213.9 0.1 copy.75
  214.0 0.1 copy.70
  214.2 48.5 %all-to-all-done.1 = bf16[16,32,16,128]{3,2,1,0:T(8,128)(2,1)S(1)} async-done(((bf16[16,32,16,128]{3,2,1,0:T(8,128)(2,1)}), bf16[16,32,16,128]{3,2,1,0:T(8,128)(2,1)S(1)}, u32[]{:S(2)}, u32[]{:S(2)}) %all-to-all-start.1) | async-done | bytes 2097184 | tf_op jit(solution)/shard_map/all_to_all | solution.py:87
  262.6 0.9 reduce_sum.69
  263.6 5.3 %all-to-all-start.2 = ((bf16[32,16,128]{2,1,0:T(8,128)(2,1)}), bf16[32,16,128]{2,1,0:T(8,128)(2,1)S(1)}, u32[]{:S(2)}, u32[]{:S(2)}) async-start(bf16[32,16,128]{2,1,0:T(8,128)(2,1)} %reduce_sum.69), calls=%async_computation.2 | async-start | bytes 262144 | tf_op jit(solution)/shard_map/all_to_all | solution.py:256
  268.9 9.4 %all-to-all-done.2 = bf16[32,16,128]{2,1,0:T(8,128)(2,1)S(1)} async-done(((bf16[32,16,128]{2,1,0:T(8,128)(2,1)}), bf16[32,16,128]{2,1,0:T(8,128)(2,1)S(1)}, u32[]{:S(2)}, u32[]{:S(2)}) %all-to-all-start.2) | async-done | bytes 131104 | tf_op jit(solution)/shard_map/all_to_all | solution.py:256
  278.3 0.9 gather_fusion
  279.2 0.3 multiply_reduce_fusion
  279.6 0.6 add_convert_fusion
  (82 shorter events, 1.7 us)
Async XLA Ops:
  0.0 197.5 %copy-start = (bf16[1,256,2048]{2,1,0:T(8,128)(2,1)S(1)}, bf16[1,256,2048]{2,1,0:T(8,128)(2,1)}, u32[]{:S(2)}) copy-start(bf16[1,256,2048]{2,1,0:T(8,128)(2,1)} %param.39) | copy-start | bytes 3145732
  2.4 12.4 %collective-permute-start = (bf16[2,384]{1,0:T(2,128)(2,1)S(1)}, bf16[2,384]{1,0:T(2,128)(2,1)S(1)}, u32[]{:S(2)}, u32[]{:S(2)}) collective-permute-start(bf16[2,384]{1,0:T(2,128)(2,1)S(1)} %get-tuple-element.47), channel_id=1, source_target_pairs={{0,16},{16,32},{32,48},{48,64},{64,80},{80,96},{96,112},{112,128},... | collective-permute-start | bytes 4616 | tf_op jit(solution)/shard_map/ppermute | solution.py:25
  6.3 8.4 %collective-permute-start.1 = (bf16[2,384]{1,0:T(2,128)(2,1)S(1)}, bf16[2,384]{1,0:T(2,128)(2,1)S(1)}, u32[]{:S(2)}, u32[]{:S(2)}) collective-permute-start(bf16[2,384]{1,0:T(2,128)(2,1)S(1)} %get-tuple-element.48), channel_id=1, source_target_pairs={{16,0},{32,16},{48,32},{64,48},{80,64},{96,80},{112,96},{128,112},... | collective-permute-start | bytes 4616 | tf_op jit(solution)/shard_map/ppermute | solution.py:27
  82.7 1.9 copy-start.2
  82.7 2.0 copy-start.7
  82.7 40.0 %copy-start.1 = (bf16[2048,128]{1,0:T(8,128)(2,1)S(1)}, bf16[2048,128]{1,0:T(8,128)(2,1)}, u32[]{:S(2)}) copy-start(bf16[2048,128]{1,0:T(8,128)(2,1)} %param.32) | copy-start | bytes 1572868
  82.7 40.0 %copy-start.3 = (bf16[128,128]{1,0:T(8,128)(2,1)S(1)}, bf16[128,128]{1,0:T(8,128)(2,1)}, u32[]{:S(2)}) copy-start(bf16[128,128]{1,0:T(8,128)(2,1)} %param.20) | copy-start | bytes 98308
  83.9 55.7 %copy-start.5 = (f32[2048]{0:T(1024)S(1)}, f32[2048]{0:T(1024)}, u32[]{:S(2)}) copy-start(f32[2048]{0:T(1024)} %param.33) | copy-start | bytes 24580
  140.4 55.6 %copy-start.9 = (bf16[1,2048,256]{2,1,0:T(8,128)(2,1)S(1)}, bf16[1,2048,256]{2,1,0:T(8,128)(2,1)}, u32[]{:S(2)}) copy-start(bf16[1,2048,256]{2,1,0:T(8,128)(2,1)} %param.37) | copy-start | bytes 3145732
  206.7 6.9 %copy-start.4 = (s32[128,2]{0,1:T(2,128)S(1)}, s32[128,2]{0,1:T(2,128)}, u32[]{:S(2)}) copy-start(s32[128,2]{0,1:T(2,128)} %param.34) | copy-start | bytes 3076
  206.7 7.3 %copy-start.6 = (f32[128,2]{0,1:T(2,128)S(1)}, f32[128,2]{0,1:T(2,128)}, u32[]{:S(2)}) copy-start(f32[128,2]{0,1:T(2,128)} %param.36) | copy-start | bytes 3076
  206.7 7.4 %copy-start.8 = (f32[128]{0:T(128)S(1)}, f32[128]{0:T(128)}, u32[]{:S(2)}) copy-start(f32[128]{0:T(128)} %param.35) | copy-start | bytes 1540
  206.7 56.0 %all-to-all-start.1 = ((bf16[16,32,16,128]{3,2,1,0:T(8,128)(2,1)}), bf16[16,32,16,128]{3,2,1,0:T(8,128)(2,1)S(1)}, u32[]{:S(2)}, u32[]{:S(2)}) async-start(bf16[16,32,16,128]{3,2,1,0:T(8,128)(2,1)} %bitcast.251), calls=%async_computation.1 | async-start | bytes 4194304 | tf_op jit(solution)/shard_map/all_to_all | solution.py:87
  263.6 14.8 %all-to-all-start.2 = ((bf16[32,16,128]{2,1,0:T(8,128)(2,1)}), bf16[32,16,128]{2,1,0:T(8,128)(2,1)S(1)}, u32[]{:S(2)}, u32[]{:S(2)}) async-start(bf16[32,16,128]{2,1,0:T(8,128)(2,1)} %reduce_sum.69), calls=%async_computation.2 | async-start | bytes 262144 | tf_op jit(solution)/shard_map/all_to_all | solution.py:256
where the time goes:
time: 281 us; the launch traced here: 280 us
  blocking collectives  175 us (62%)
  waiting for transfers between devices  57.9 us (21%)
  starting transfers between devices  17.4 us (6%)
  local copies, waits for them, and re-layouts  13.4 us (5%)
  matrix products  9.61 us (3%)
  other arithmetic  6.01 us (2%)
    all_gather x4, blocking collectives, all_in_one(): both, at, found = (lax.all_gather(jnp.concatenate(lines), axis), 0, {})  65.3 us
    all_to_all x1, blocking collectives, body(): lax.all_to_all(outgoing, SP, split_axis=0, concat_axis=0, tiled=True)  55.6 us
    all_to_all x1, waiting for transfers between devices, sum_at_owner(): parts = lax.all_to_all(in_blocks(shard, dim, peers), axis, 0, 0, tiled=True)  48.5 us
    all_gather x1, blocking collectives, body(): lax.all_gather(mixed, 'tp', axis=1, tiled=True)  37.9 us
    all_gather x1, blocking collectives, body(): lax.all_gather(stream, 'tp', axis=1, tiled=True).astype(jnp.float32)  16.4 us
    all_to_all x1, waiting for transfers between devices, body(): lax.all_to_all(expert_cols, SP, split_axis=0, concat_axis=0, tiled=True)  9.43 us
    all_to_all x1, starting transfers between devices, sum_at_owner(): parts = lax.all_to_all(in_blocks(shard, dim, peers), axis, 0, 0, tiled=True)  6.91 us
    unnamed x30, local copies, waits for them, and re-layouts  6.06 us
  transfers between devices with their start and end apart: 4, of which 2 were waited for; matrix products, arithmetic and copies ran while one was open for 3% of the time, Pallas kernels for 0%

commit v1 on v0

--- a/solution.py
+++ b/solution.py
@@ -12,6 +12,12 @@
 HIGHEST = lax.Precision.HIGHEST
 group_eps = 1e-05
 stream_eps = 1e-06
+
+
+def gather_from_all(x, axis, dim):
+    length = lax.axis_size(axis)
+    repeats = [length if d == dim else 1 for d in range(x.ndim)]
+    return lax.all_to_all(jnp.tile(x, repeats), axis, split_axis=dim, concat_axis=dim, tiled=True)
 
 
 def extended(cells, sides, width):
@@ -210,7 +216,7 @@
     grouped = grouped * lax.rsqrt(jnp.mean(grouped * grouped, axis=-1, keepdims=True) + group_eps)
     mixed = (grouped.reshape(tokens_here, x_width) * clustered_rescale_factor).astype(jnp.bfloat16)
     projected = jnp.dot(
-        lax.all_gather(mixed, "tp", axis=1, tiled=True),
+        gather_from_all(mixed, "tp", 1),
         final_projection_weights,
         preferred_element_type=jnp.float32,
     )

time: 281 us -> 284 us (1.011)
  blocking collectives: 175 us -> 137 us
  starting transfers between devices: 17.4 us -> 43.4 us
  waiting for transfers between devices: 57.9 us -> 73.5 us
    all_gather x1 -> x0, blocking collectives: 37.9 us -> none  [body(): lax.all_gather(mixed, 'tp', axis=1, tiled=True)]
    all_to_all x0 -> x1, starting transfers between devices: none -> 25.8 us  [gather_from_all(): lax.all_to_all(jnp.tile(x, repeats), axis, split_axis=dim, concat_axis=di...]
    all_to_all x0 -> x1, waiting for transfers between devices: none -> 15.5 us  [gather_from_all(): lax.all_to_all(jnp.tile(x, repeats), axis, split_axis=dim, concat_axis=di...]
  transfers between devices with their start and end apart: 4 -> 5, of which waited for: 2 -> 3; matrix products, arithmetic and copies ran while one was open for 3% -> 2% of each run, Pallas kernels for 0% -> 0%
where the time goes in v1:
time: 284 us
  blocking collectives  137 us (48%)
  waiting for transfers between devices  73.5 us (26%)
  starting transfers between devices  43.4 us (15%)
  local copies, waits for them, and re-layouts  13.9 us (5%)
  matrix products  9.69 us (3%)
  other arithmetic  5.32 us (2%)
    all_gather x4, blocking collectives, all_in_one(): both, at, found = (lax.all_gather(jnp.concatenate(lines), axis), 0, {})  65.6 us
    all_to_all x1, blocking collectives, body(): lax.all_to_all(outgoing, SP, split_axis=0, concat_axis=0, tiled=True)  55.7 us
    all_to_all x1, waiting for transfers between devices, sum_at_owner(): parts = lax.all_to_all(in_blocks(shard, dim, peers), axis, 0, 0, tiled=True)  48.5 us
    all_to_all x1, starting transfers between devices, gather_from_all(): lax.all_to_all(jnp.tile(x, repeats), axis, split_axis=dim, concat_axis=di...  25.8 us
    all_gather x1, blocking collectives, body(): lax.all_gather(stream, 'tp', axis=1, tiled=True).astype(jnp.float32)  15.9 us
    all_to_all x1, waiting for transfers between devices, gather_from_all(): lax.all_to_all(jnp.tile(x, repeats), axis, split_axis=dim, concat_axis=di...  15.5 us
    all_to_all x1, waiting for transfers between devices, body(): lax.all_to_all(expert_cols, SP, split_axis=0, concat_axis=0, tiled=True)  9.43 us
    all_to_all x1, starting transfers between devices, sum_at_owner(): parts = lax.all_to_all(in_blocks(shard, dim, peers), axis, 0, 0, tiled=True)  7.09 us
  transfers between devices with their start and end apart: 5, of which 3 were waited for; matrix products, arithmetic and copies ran while one was open for 2% of the time, Pallas kernels for 0%

profile of v1, /device:TPU:1, one launch (start us, length us, event | category | flops | bytes accessed | tf_op | source)
XLA Modules:
  0.0 283.6 jit_solution(14853893391327299424)
XLA Ops:
  0.0 0.9 constant_dynamic-update-slice_fusion.5
  0.9 0.8 constant_dynamic-update-slice_fusion.4
  1.6 0.8 constant_dynamic-update-slice_fusion.3
  2.4 3.9 %collective-permute-start = (bf16[2,384]{1,0:T(2,128)(2,1)S(1)}, bf16[2,384]{1,0:T(2,128)(2,1)S(1)}, u32[]{:S(2)}, u32[]{:S(2)}) collective-permute-start(bf16[2,384]{1,0:T(2,128)(2,1)S(1)} %get-tuple-element.47), channel_id=1, source_target_pairs={{0,16},{16,32},{32,48},{48,64},{64,80},{80,96},{96,112},{112,128},... | collective-permute-start | bytes 4616 | tf_op jit(solution)/shard_map/ppermute | solution.py:31
  6.3 1.3 collective-permute-start.1
  7.7 0.8 multiply_add_fusion
  8.5 0.1 rev.7
  8.6 0.3 reduce_window_sum.30
  8.9 0.3 reduce_window_sum.31
  9.2 0.1 rev.8
  9.3 0.2 slice_reduce_fusion.6
  9.6 0.7 constant_dynamic-update-slice_fusion.2
  10.3 0.7 constant_dynamic-update-slice_fusion.1
  11.0 0.7 constant_dynamic-update-slice_fusion
  11.8 0.2 multiply_convert_fusion
  12.0 0.1 copy.78
  12.1 0.2 convolution_convert_fusion.2
  12.4 10.7 %all-gather.6 = bf16[4,129,128]{2,1,0:T(8,128)(2,1)S(1)} all-gather(bf16[1,129,128]{2,1,0:T(8,128)(2,1)S(1)} %maximum_bitcast_fusion.2), channel_id=4, replica_groups=mesh['sp_0'=8,'sp_1'=4,'tp'=16] {'sp_1'}, dimensions={0}, use_global_device_ids=true | all-gather | bytes 165120 | tf_op jit(solution)/shard_map/all_gather | solution.py:54
  23.4 0.1 mul.549
  23.8 0.1 fusion.71
  23.9 27.0 %all-gather.7 = bf16[8,129,128]{2,1,0:T(8,128)(2,1)S(1)} all-gather(bf16[1,129,128]{2,1,0:T(8,128)(2,1)S(1)} %maximum_bitcast_fusion.3), channel_id=5, replica_groups=mesh['sp_0'=8,'sp_1'=4,'tp'=16] {'sp_0'}, dimensions={0}, use_global_device_ids=true | all-gather | bytes 297216 | tf_op jit(solution)/shard_map/all_gather | solution.py:54
  51.0 0.2 convolution_convert_fusion.3
  51.2 9.1 %all-gather.4 = bf16[4,129,128]{2,1,0:T(8,128)(2,1)S(1)} all-gather(bf16[1,129,128]{2,1,0:T(8,128)(2,1)S(1)} %maximum_bitcast_fusion), channel_id=2, replica_groups=mesh['sp_0'=8,'sp_1'=4,'tp'=16] {'sp_1'}, dimensions={0}, use_global_device_ids=true | all-gather | bytes 165120 | tf_op jit(solution)/shard_map/all_gather | solution.py:54
  61.0 0.1 fusion.75
  61.2 18.8 %all-gather.5 = bf16[8,129,128]{2,1,0:T(8,128)(2,1)S(1)} all-gather(bf16[1,129,128]{2,1,0:T(8,128)(2,1)S(1)} %maximum_bitcast_fusion.1), channel_id=3, replica_groups=mesh['sp_0'=8,'sp_1'=4,'tp'=16] {'sp_0'}, dimensions={0}, use_global_device_ids=true | all-gather | bytes 297216 | tf_op jit(solution)/shard_map/all_gather | solution.py:54
  80.0 0.1 fusion.184
  80.3 0.4 convolution_bitcast_fusion.2
  80.7 0.5 fusion.5
  81.2 0.5 fusion.3
  81.8 0.1 copy.81
  81.9 0.1 multiply_reduce_fusion.1
  82.0 0.1 multiply_convert_fusion.1
  82.1 0.9 tile.2
  83.0 25.8 %all-to-all-start = ((bf16[128,16,128]{2,0,1:T(8,128)(2,1)}), bf16[128,16,128]{2,0,1:T(8,128)(2,1)S(1)}, u32[]{:S(2)}, u32[]{:S(2)}) async-start(bf16[128,16,128]{2,0,1:T(8,128)(2,1)} %tile.2), calls=%async_computation | async-start | bytes 1048576 | tf_op jit(solution)/shard_map/all_to_all | solution.py:20
  108.8 0.1 copy.84
  108.9 0.1 eq.27
  109.1 0.1 reshape.654
  109.2 0.6 reduce-window.6
  109.8 0.2 slice_reduce_fusion
  110.1 0.1 fusion.128
  110.2 0.1 reduce_sum.66
  110.5 15.5 %all-to-all-done = bf16[128,16,128]{2,0,1:T(8,128)(2,1)S(1)} async-done(((bf16[128,16,128]{2,0,1:T(8,128)(2,1)}), bf16[128,16,128]{2,0,1:T(8,128)(2,1)S(1)}, u32[]{:S(2)}, u32[]{:S(2)}) %all-to-all-start) | async-done | bytes 524320 | tf_op jit(solution)/shard_map/all_to_all | solution.py:20
  126.0 0.3 copy.82
  126.3 0.3 fusion.6
  126.7 15.9 %all_gather.35 = bf16[128,2048]{1,0:T(8,128)(2,1)S(1)} all-gather(bf16[128,128]{1,0:T(8,128)(2,1)S(1)} %fusion.6), channel_id=1, replica_groups=mesh['sp_0'=8,'sp_1'=4,'tp'=16] {'tp'}, dimensions={1}, use_global_device_ids=true | all-gather | bytes 557056 | tf_op jit(solution)/shard_map/all_gather | solution.py:226
  142.6 0.2 fusion.7
  142.8 0.8 convolution_convert_fusion.1
  143.6 55.7 %all_to_all.24 = bf16[32,16,2048]{2,1,0:T(8,128)(2,1)S(1)} all-to-all(bf16[32,16,2048]{2,1,0:T(8,128)(2,1)S(1)} %bitcast.253), channel_id=1, replica_groups=mesh['sp_0'=8,'sp_1'=4,'tp'=16] {'sp_0','sp_1'}, dimensions={0} | all-to-all | bytes 4194304 | tf_op jit(solution)/shard_map/all_to_all | solution.py:250
  199.3 1.5 fusion.12
  200.8 5.0 %fusion = bf16[64,8,16,128]{3,1,2,0:T(8,128)(2,1)} fusion(bf16[1,256,2048]{2,1,0:T(8,128)(2,1)S(1)} %copy-done, bf16[512,2048]{1,0:T(8,128)(2,1)S(1)} %bitcast.257, bf16[1,2048,256]{2,1,0:T(8,128)(2,1)} %param.38, f32[512,256]{1,0:T(8,128)} %fusion.12), kind=kOutput, calls=%fused_computation.4 | convolution fusion | flops 1075576832 | bytes 6815744 | tf_op jit(solution)/shard_map/dot_general | solution.py:257
  205.8 2.2 copy.96
  208.0 1.9 copy.103
  209.9 7.1 %all-to-all-start.2 = ((bf16[16,32,16,128]{3,2,1,0:T(8,128)(2,1)}), bf16[16,32,16,128]{3,2,1,0:T(8,128)(2,1)S(1)}, u32[]{:S(2)}, u32[]{:S(2)}) async-start(bf16[16,32,16,128]{3,2,1,0:T(8,128)(2,1)} %bitcast.252), calls=%async_computation.2 | async-start | bytes 4194304 | tf_op jit(solution)/shard_map/all_to_all | solution.py:93
  217.0 0.1 copy.90
  217.1 0.1 mul.606
  217.3 0.1 copy.88
  217.5 0.1 copy.83
  217.6 48.5 %all-to-all-done.2 = bf16[16,32,16,128]{3,2,1,0:T(8,128)(2,1)S(1)} async-done(((bf16[16,32,16,128]{3,2,1,0:T(8,128)(2,1)}), bf16[16,32,16,128]{3,2,1,0:T(8,128)(2,1)S(1)}, u32[]{:S(2)}, u32[]{:S(2)}) %all-to-all-start.2) | async-done | bytes 2097184 | tf_op jit(solution)/shard_map/all_to_all | solution.py:93
  266.1 0.9 reduce_sum.69
  267.0 5.3 %all-to-all-start.3 = ((bf16[32,16,128]{2,1,0:T(8,128)(2,1)}), bf16[32,16,128]{2,1,0:T(8,128)(2,1)S(1)}, u32[]{:S(2)}, u32[]{:S(2)}) async-start(bf16[32,16,128]{2,1,0:T(8,128)(2,1)} %reduce_sum.69), calls=%async_computation.3 | async-start | bytes 262144 | tf_op jit(solution)/shard_map/all_to_all | solution.py:262
  272.4 9.4 %all-to-all-done.3 = bf16[32,16,128]{2,1,0:T(8,128)(2,1)S(1)} async-done(((bf16[32,16,128]{2,1,0:T(8,128)(2,1)}), bf16[32,16,128]{2,1,0:T(8,128)(2,1)S(1)}, u32[]{:S(2)}, u32[]{:S(2)}) %all-to-all-start.3) | async-done | bytes 131104 | tf_op jit(solution)/shard_map/all_to_all | solution.py:262
  281.8 0.9 gather_fusion
  282.6 0.3 multiply_reduce_fusion
  283.0 0.6 add_convert_fusion
  (85 shorter events, 1.9 us)
Async XLA Ops:
  0.0 200.8 %copy-start = (bf16[1,256,2048]{2,1,0:T(8,128)(2,1)S(1)}, bf16[1,256,2048]{2,1,0:T(8,128)(2,1)}, u32[]{:S(2)}) copy-start(bf16[1,256,2048]{2,1,0:T(8,128)(2,1)} %param.39) | copy-start | bytes 3145732
  2.4 9.4 %collective-permute-start = (bf16[2,384]{1,0:T(2,128)(2,1)S(1)}, bf16[2,384]{1,0:T(2,128)(2,1)S(1)}, u32[]{:S(2)}, u32[]{:S(2)}) collective-permute-start(bf16[2,384]{1,0:T(2,128)(2,1)S(1)} %get-tuple-element.47), channel_id=1, source_target_pairs={{0,16},{16,32},{32,48},{48,64},{64,80},{80,96},{96,112},{112,128},... | collective-permute-start | bytes 4616 | tf_op jit(solution)/shard_map/ppermute | solution.py:31
  6.3 5.5 %collective-permute-start.1 = (bf16[2,384]{1,0:T(2,128)(2,1)S(1)}, bf16[2,384]{1,0:T(2,128)(2,1)S(1)}, u32[]{:S(2)}, u32[]{:S(2)}) collective-permute-start(bf16[2,384]{1,0:T(2,128)(2,1)S(1)} %get-tuple-element.48), channel_id=1, source_target_pairs={{16,0},{32,16},{48,32},{64,48},{80,64},{96,80},{112,96},{128,112},... | collective-permute-start | bytes 4616 | tf_op jit(solution)/shard_map/ppermute | solution.py:33
  80.0 1.9 copy-start.2
  80.0 2.0 copy-start.7
  80.7 28.1 %copy-start.4 = (s32[128,2]{0,1:T(2,128)S(1)}, s32[128,2]{0,1:T(2,128)}, u32[]{:S(2)}) copy-start(s32[128,2]{0,1:T(2,128)} %param.34) | copy-start | bytes 3076
  81.2 45.1 %copy-start.1 = (bf16[2048,128]{1,0:T(8,128)(2,1)S(1)}, bf16[2048,128]{1,0:T(8,128)(2,1)}, u32[]{:S(2)}) copy-start(bf16[2048,128]{1,0:T(8,128)(2,1)} %param.32) | copy-start | bytes 1572868
  81.2 45.1 %copy-start.3 = (bf16[128,128]{1,0:T(8,128)(2,1)S(1)}, bf16[128,128]{1,0:T(8,128)(2,1)}, u32[]{:S(2)}) copy-start(bf16[128,128]{1,0:T(8,128)(2,1)} %param.20) | copy-start | bytes 98308
  83.0 43.0 %all-to-all-start = ((bf16[128,16,128]{2,0,1:T(8,128)(2,1)}), bf16[128,16,128]{2,0,1:T(8,128)(2,1)S(1)}, u32[]{:S(2)}, u32[]{:S(2)}) async-start(bf16[128,16,128]{2,0,1:T(8,128)(2,1)} %tile.2), calls=%async_computation | async-start | bytes 1048576 | tf_op jit(solution)/shard_map/all_to_all | solution.py:20
  108.8 34.0 %copy-start.5 = (f32[2048]{0:T(1024)S(1)}, f32[2048]{0:T(1024)}, u32[]{:S(2)}) copy-start(f32[2048]{0:T(1024)} %param.33) | copy-start | bytes 24580
  143.6 55.7 %copy-start.9 = (bf16[1,2048,256]{2,1,0:T(8,128)(2,1)S(1)}, bf16[1,2048,256]{2,1,0:T(8,128)(2,1)}, u32[]{:S(2)}) copy-start(bf16[1,2048,256]{2,1,0:T(8,128)(2,1)} %param.37) | copy-start | bytes 3145732
  209.9 7.5 %copy-start.6 = (f32[128,2]{0,1:T(2,128)S(1)}, f32[128,2]{0,1:T(2,128)}, u32[]{:S(2)}) copy-start(f32[128,2]{0,1:T(2,128)} %param.36) | copy-start | bytes 3076
  209.9 7.5 %copy-start.8 = (f32[128]{0:T(128)S(1)}, f32[128]{0:T(128)}, u32[]{:S(2)}) copy-start(f32[128]{0:T(128)} %param.35) | copy-start | bytes 1540
  209.9 56.1 %all-to-all-start.2 = ((bf16[16,32,16,128]{3,2,1,0:T(8,128)(2,1)}), bf16[16,32,16,128]{3,2,1,0:T(8,128)(2,1)S(1)}, u32[]{:S(2)}, u32[]{:S(2)}) async-start(bf16[16,32,16,128]{3,2,1,0:T(8,128)(2,1)} %bitcast.252), calls=%async_computation.2 | async-start | bytes 4194304 | tf_op jit(solution)/shard_map/all_to_all | solution.py:93
  267.0 14.8 %all-to-all-start.3 = ((bf16[32,16,128]{2,1,0:T(8,128)(2,1)}), bf16[32,16,128]{2,1,0:T(8,128)(2,1)S(1)}, u32[]{:S(2)}, u32[]{:S(2)}) async-start(bf16[32,16,128]{2,1,0:T(8,128)(2,1)} %reduce_sum.69), calls=%async_computation.3 | async-start | bytes 262144 | tf_op jit(solution)/shard_map/all_to_all | solution.py:262
